TPU v7x, 32 devices: a whole 2x2x4 slice. The times are simulated.
32 devices in a mesh: sp: 8 (over z, y), tp: 4 (over x, core).
Axes of the slice: x: 2, y: 2, z: 4, core: 2. Of those that a mesh axis runs over, the one named last changes fastest.
Arguments:
- queries: bfloat16 [4096, 2048], P('sp', 'tp'), may hold values from -6 to 6
- keys: bfloat16 [4096, 512], P('sp', 'tp'), may hold values from -6 to 6
- values: bfloat16 [4096, 512], P('sp', 'tp'), may hold values from -6 to 6
- residual: bfloat16 [4096, 2048], P(('sp', 'tp')), may hold values from -0.119628906 to 0.119628906
- out_proj: bfloat16 [2048, 2048], replicated, may hold values from -0.125 to 0.125
- query_gain: float32 [128], replicated, may hold values from 0.7 to 7
- key_gain: float32 [128], replicated, may hold values from 0.7 to 7
- norm_gain: float32 [2048], replicated, may hold values from 0.1 to 1.9
- routes: int32 [4096, 4], P(('sp', 'tp')), may hold values from 0 to 31, all different within a row; in each aligned block of 128 rows (0 to 127, 128 to 255, ...) at most 32 rows name the same one
- route_weight: float32 [4096, 4], P(('sp', 'tp')), may hold values from 0.1 to 1
- expert_gate: bfloat16 [32, 2048, 256], P(('sp', 'tp')), may hold values from -0.125 to 0.125
- expert_up: bfloat16 [32, 2048, 256], P(('sp', 'tp')), may hold values from -0.125 to 0.125
- expert_down: bfloat16 [32, 256, 2048], P(('sp', 'tp')), may hold values from -0.375 to 0.375
- shared_gate: bfloat16 [2048, 256], replicated, may hold values from -0.125 to 0.125
- shared_up: bfloat16 [2048, 256], replicated, may hold values from -0.125 to 0.125
- shared_down: bfloat16 [256, 2048], replicated, may hold values from -0.375 to 0.375
Outputs:
- layer_out: bfloat16 [4096, 2048], P(('sp', 'tp'))
Inputs may be any that keep to these rules, and one draw needn't show every extreme that they name: In the rows of one device (aligned blocks of 128 tokens), no expert is named by more than 32 routes; some expert is named by exactly 32 routes of some device; the 4 experts of a token differ.
All inputs are finite; a program needn't handle non-finite values.
Results may differ from a plain program's by a relative error of at most 0.023.
The roundings to bfloat16 on the way count: a program that leaves them out, or rounds other values in their place, can miss the bound.
Values may be sent and summed in bfloat16 or wider, within the bound.
A program may use at most 128 MiB of HBM per device.

v0:
```python
import math

import jax
import jax.numpy as jnp
from jax import lax
from jax.sharding import PartitionSpec as P

HEADS = 16
KV_HEADS = 4
GRID_W = 64


EPS = 1e-06
THETA = 10000.0


def rotate_pairs(block, cosine, sine):
    first, second = jnp.split(block, 2, axis=-1)
    return jnp.concatenate(
        [first * cosine - second * sine, second * cosine + first * sine], axis=-1
    )


def normed_rotary(source, gain, heads, offset):
    count = source.shape[0]
    width = gain.shape[0]
    values_f = source.astype(jnp.float32).reshape(count, heads, width)
    values_f = (
        values_f * lax.rsqrt(jnp.mean(values_f * values_f, axis=-1, keepdims=True) + EPS) * gain
    )
    position = offset + jnp.arange(count, dtype=jnp.int32)
    grid_row = (position // GRID_W).astype(jnp.float32)
    grid_col = (position % GRID_W).astype(jnp.float32)
    quarter = width // 4
    inverse = jnp.power(THETA, -4.0 * jnp.arange(quarter, dtype=jnp.float32) / width)
    row_angle = (grid_row[:, None] * inverse[None, :])[:, None, :]
    col_angle = (grid_col[:, None] * inverse[None, :])[:, None, :]
    row_half, col_half = jnp.split(values_f, 2, axis=-1)
    turned = jnp.concatenate(
        [
            rotate_pairs(row_half, jnp.cos(row_angle), jnp.sin(row_angle)),
            rotate_pairs(col_half, jnp.cos(col_angle), jnp.sin(col_angle)),
        ],
        axis=-1,
    )
    return turned.reshape(count, heads * width).astype(jnp.bfloat16)


def expert_apply(arrived, expert_gate, expert_up, expert_down):
    sources, slots, width = arrived.shape
    local = expert_gate.shape[0]
    grouped = arrived.reshape(sources // local, local, slots, width)
    gate_part = jnp.einsum(
        "sech,ehf->secf", grouped, expert_gate, preferred_element_type=jnp.float32
    )
    up_part = jnp.einsum("sech,ehf->secf", grouped, expert_up, preferred_element_type=jnp.float32)
    hidden_e = (jax.nn.silu(gate_part) * up_part).astype(jnp.bfloat16)
    result = jnp.einsum("secf,efh->sech", hidden_e, expert_down, preferred_element_type=jnp.float32)
    return result.astype(jnp.bfloat16).reshape(sources, slots, width)


def body(
    queries,
    keys,
    values,
    residual,
    out_proj,
    query_gain,
    key_gain,
    norm_gain,
    routes,
    route_weight,
    expert_gate,
    expert_up,
    expert_down,
    shared_gate,
    shared_up,
    shared_down,
):
    tok_local = queries.shape[0]
    width = query_gain.shape[0]
    group = HEADS // KV_HEADS
    kv_local = keys.shape[1] // width
    scale = 1.0 / math.sqrt(width)
    offset = lax.axis_index("sp") * tok_local
    q_rot = normed_rotary(queries, query_gain, kv_local * group, offset)
    k_rot = normed_rotary(keys, key_gain, kv_local, offset)
    query_3d = q_rot.reshape(tok_local, kv_local, group, width).transpose(1, 2, 0, 3)
    query_3d = query_3d.reshape(kv_local, group * tok_local, width)
    start_state = (
        jnp.full((kv_local, group * tok_local), -jnp.inf, jnp.float32),
        jnp.zeros((kv_local, group * tok_local), jnp.float32),
        jnp.zeros((kv_local, group * tok_local, width), jnp.float32),
    )
    key_piece = lax.all_gather(k_rot, "sp", axis=0, tiled=True)
    value_piece = lax.all_gather(values, "sp", axis=0, tiled=True)
    count = key_piece.shape[0]
    block = math.gcd(count, 512)

    def one_block(index_block, state):
        running_max, running_sum, accum = state
        key_rows = lax.dynamic_slice_in_dim(key_piece, index_block * block, block, 0)
        value_rows = lax.dynamic_slice_in_dim(value_piece, index_block * block, block, 0)
        key_3d = key_rows.reshape(block, kv_local, width)
        value_3d = value_rows.reshape(block, kv_local, width)
        scores = (
            jnp.einsum("gqd,kgd->gqk", query_3d, key_3d, preferred_element_type=jnp.float32) * scale
        )
        new_max = jnp.maximum(running_max, jnp.max(scores, axis=-1))
        weights = jnp.exp(scores - new_max[..., None])
        factor = jnp.exp(running_max - new_max)
        new_sum = running_sum * factor + jnp.sum(weights, axis=-1)
        added = jnp.einsum(
            "gqk,kgd->gqd",
            weights.astype(jnp.bfloat16),
            value_3d,
            preferred_element_type=jnp.float32,
        )
        return (new_max, new_sum, accum * factor[..., None] + added)

    final_max, final_sum, final_acc = lax.fori_loop(0, count // block, one_block, start_state)
    attn_local = (final_acc / final_sum[..., None]).astype(jnp.bfloat16)
    attn_local = attn_local.reshape(kv_local, group, tok_local, width).transpose(2, 0, 1, 3)
    attn_local = attn_local.reshape(tok_local, kv_local * group * width)
    all_heads = lax.all_to_all(attn_local, "tp", split_axis=0, concat_axis=1, tiled=True)
    projected = jnp.dot(all_heads, out_proj, preferred_element_type=jnp.float32)
    hidden1 = (residual.astype(jnp.float32) + projected).astype(jnp.bfloat16)
    hidden_f = hidden1.astype(jnp.float32)
    normed = (
        hidden_f
        * lax.rsqrt(jnp.mean(hidden_f * hidden_f, axis=-1, keepdims=True) + EPS)
        * norm_gain
    ).astype(jnp.bfloat16)
    rows_local = normed.shape[0]
    top_count = routes.shape[1]
    pair_count = rows_local * top_count
    expert_total = expert_gate.shape[0] * lax.axis_size("sp") * lax.axis_size("tp")
    capacity = max(2, 2 * rows_local * top_count // expert_total)
    flat_routes = routes.reshape(pair_count)
    one_hot = (flat_routes[:, None] == jnp.arange(expert_total, dtype=jnp.int32)[None, :]).astype(
        jnp.float32
    )
    lower = (jnp.arange(pair_count)[:, None] >= jnp.arange(pair_count)[None, :]).astype(jnp.float32)
    running_count = jnp.dot(lower, one_hot, precision=lax.Precision.HIGHEST)
    slot_place = (jnp.sum(running_count * one_hot, axis=1) - 1.0).astype(jnp.int32)
    slot_index = flat_routes * capacity + slot_place
    slot_total = expert_total * capacity
    placement = (jnp.arange(slot_total, dtype=jnp.int32)[:, None] == slot_index[None, :]).astype(
        jnp.bfloat16
    )
    placement = jnp.sum(placement.reshape(slot_total, rows_local, top_count), axis=2)
    send_rows = jnp.dot(placement, normed, preferred_element_type=jnp.float32).astype(jnp.bfloat16)
    send_rows = send_rows.reshape(expert_total, capacity, normed.shape[1])
    shared_hidden = (
        jax.nn.silu(jnp.dot(normed, shared_gate, preferred_element_type=jnp.float32))
        * jnp.dot(normed, shared_up, preferred_element_type=jnp.float32)
    ).astype(jnp.bfloat16)
    shared_out = jnp.dot(shared_hidden, shared_down, preferred_element_type=jnp.float32)
    processed = expert_apply(
        lax.all_to_all(send_rows, ("sp", "tp"), split_axis=0, concat_axis=0, tiled=True),
        expert_gate,
        expert_up,
        expert_down,
    )
    returned = lax.all_to_all(processed, ("sp", "tp"), split_axis=0, concat_axis=0, tiled=True)
    returned = returned.reshape(slot_total, normed.shape[1])
    routed = (
        returned[slot_index].reshape(rows_local, top_count, normed.shape[1]).astype(jnp.float32)
    )
    mixed = jnp.einsum("tk,tkd->td", route_weight, routed) + shared_out
    return (hidden_f + mixed).astype(jnp.bfloat16)


def solution(mesh):
    placed = (
        P("sp", "tp"),
        P("sp", "tp"),
        P("sp", "tp"),
        P(("sp", "tp"), None),
        P(),
        P(),
        P(),
        P(),
        P(("sp", "tp"), None),
        P(("sp", "tp"), None),
        P(("sp", "tp"), None, None),
        P(("sp", "tp"), None, None),
        P(("sp", "tp"), None, None),
        P(),
        P(),
        P(),
    )
    return jax.shard_map(
        body, mesh=mesh, in_specs=placed, out_specs=P(("sp", "tp"), None), check_vma=False
    )
```

profile of v0, /device:TPU:0, one launch (start us, length us, event | category | flops | bytes accessed | tf_op | source)
XLA Modules:
  0.0 420.8 jit_solution(3090994777994951920)
XLA Ops:
  6.6 1.1 copy.35
  7.7 0.7 fusion.43
  8.5 0.6 fusion.62
  9.0 0.7 pad_maximum_fusion
  9.8 0.7 all-gather.4.cloned.1.call-update
  10.5 1.4 reshape.480
  11.9 0.6 multiply_reduce_fusion.2
  12.6 1.9 multiply_cosine_fusion.1
  14.5 0.7 multiply_multiply_fusion
  15.2 1.8 fusion.37
  17.0 1.6 maximum_bitcast_fusion
  19.2 32.9 %all-gather.6.cloned.1.call-done = bf16[4096,1,128]{0,2,1:T(8,128)(2,1)} async-done(((bf16[512,1,128]{0,2,1:T(8,128)(2,1)}), bf16[4096,1,128]{0,2,1:T(8,128)(2,1)}) %all-gather.6.cloned.1.call-update) | async-done | bytes 1048592 | tf_op jit(solution)/shard_map/all_gather | solution.py:95
  52.1 41.4 %all-gather.4.cloned.1.call-done = bf16[4096,128]{1,0:T(8,128)(2,1)} async-done(((bf16[512,128]{1,0:T(8,128)(2,1)}), bf16[4096,128]{1,0:T(8,128)(2,1)}) %all-gather.4.cloned.1.call-update) | async-done | bytes 1048592 | tf_op jit(solution)/shard_map/all_gather | solution.py:96
  93.6 73.7 %while.18 = (s32[]{:T(128)}, f32[1,2048]{1,0:T(1,128)S(1)}, f32[1,2048]{1,0:T(1,128)S(1)}, f32[1,2048,128]{2,1,0:T(8,128)S(1)}, bf16[4096,128]{0,1:T(8,128)(2,1)...) while((s32[]{:T(128)}, f32[1,2048]{1,0:T(1,128)S(1)}, ...), condition=%wide.region_5.6_spmd.clone, body=%wide.region_2.5_spmd.clone.sunk | while | flops 546056192 | bytes 32374984 | solution.py:121
  93.6 3.6 multiply_reduce_fusion.4
  97.2 3.0 fusion.96
  100.3 0.3 copy-done.1
  100.6 2.1 fusion.98
  102.8 3.6 multiply_reduce_fusion.4
  106.4 3.0 fusion.96
  109.5 0.3 copy-done.1
  109.8 2.1 fusion.98
  112.0 3.6 multiply_reduce_fusion.4
  115.6 3.0 fusion.96
  118.7 0.3 copy-done.1
  119.0 2.1 fusion.98
  121.2 3.6 multiply_reduce_fusion.4
  124.8 3.0 fusion.96
  127.9 0.3 copy-done.1
  128.3 2.1 fusion.98
  130.4 3.6 multiply_reduce_fusion.4
  134.1 3.0 fusion.96
  137.1 0.3 copy-done.1
  137.5 2.1 fusion.98
  139.7 3.6 multiply_reduce_fusion.4
  143.3 3.0 fusion.96
  146.4 0.3 copy-done.1
  146.7 2.1 fusion.98
  148.9 3.6 multiply_reduce_fusion.4
  152.5 3.0 fusion.96
  155.6 0.3 copy-done.1
  155.9 2.1 fusion.98
  158.1 3.6 multiply_reduce_fusion.4
  161.7 3.0 fusion.96
  164.8 0.3 copy-done.1
  165.2 2.1 fusion.98
  167.3 0.3 divide_convert_fusion
  167.7 0.4 copy.51
  168.1 1.0 all_to_all.20
  169.1 3.7 all-to-all-start
  173.2 8.1 %all-to-all-done = bf16[4,128,512]{2,1,0:T(8,128)(2,1)S(1)} async-done(((bf16[4,128,512]{2,1,0:T(8,128)(2,1)}), bf16[4,128,512]{2,1,0:T(8,128)(2,1)S(1)}, u32[]{:S(2)}, u32[]{:S(2)}) %all-to-all-start) | async-done | bytes 524320 | tf_op jit(solution)/shard_map/all_to_all | solution.py:125
  181.6 4.7 %multiply_reduce_fusion.1 = (f32[128]{0:T(128)S(1)}, f32[128,2048]{1,0:T(8,128)S(1)}) fusion(bf16[128,2048]{0,1:T(8,128)(2,1)S(1)} %bitcast.106, bf16[2048,2048]{1,0:T(8,128)(2,1)} %param.22, bf16[128,2048]{1,0:T(8,128)(2,1)S(1)} %copy-done.5), kind=kOutput, calls=%fused_computation.52 | convolution fusion | flops 1075314560 | bytes 10486272 | tf_op jit(solution)/shard_map/dot_general | solution.py:126
  186.4 1.3 convolution_convert_fusion.1
  187.8 95.8 %all_to_all.29 = bf16[32,32,2048]{2,1,0:T(8,128)(2,1)S(1)} all-to-all(bf16[32,32,2048]{2,1,0:T(8,128)(2,1)S(1)} %bitcast.103), channel_id=1, replica_groups=mesh['sp'=8,'tp'=4] {'sp','tp'}, dimensions={0} | all-to-all | bytes 8388608 | tf_op jit(solution)/shard_map/all_to_all | solution.py:160
  283.6 2.0 copy-done.2
  285.6 2.3 convolution_bitcast_fusion.2
  287.9 9.1 %convolution_convert_fusion = bf16[32,32,2048]{2,1,0:T(8,128)(2,1)} fusion(bf16[32,32,2048]{2,1,0:T(8,128)(2,1)} %copy-done.2, bf16[1,256,2048]{2,1,0:T(8,128)(2,1)S(1)} %copy-done, bf16[1,2048,256]{2,1,0:T(8,128)(2,1)} %param.29, f32[32,1,32,256]{3,2,0,1:T(8,128)} %convolution_bitcast_fusion.2), kind=kOutput, calls=%fused_computation.23 | convolution fusion | flops 2151153664 | bytes 11534336 | tf_op jit(solution)/shard_map/secf,efh->sech/dot_general | solution.py:58
  297.0 4.0 all-to-all-start.2
  301.3 0.4 fusion.75
  301.7 93.0 %all-to-all-done.2 = bf16[32,32,2048]{2,1,0:T(8,128)(2,1)} async-done(((bf16[32,32,2048]{2,1,0:T(8,128)(2,1)}), bf16[32,32,2048]{2,1,0:T(8,128)(2,1)}, u32[]{:S(2)}, u32[]{:S(2)}) %all-to-all-start.2) | async-done | bytes 4194336 | tf_op jit(solution)/shard_map/all_to_all | solution.py:165
  394.7 8.0 %gather_fusion = bf16[512,2048]{1,0:T(8,128)(2,1)} fusion(bf16[1024,2048]{1,0:T(8,128)(2,1)} %bitcast.29, s32[1024]{0:T(1024)S(1)} %pad_clamp_fusion), kind=kCustom, calls=%fused_computation | custom fusion | bytes 4196352 | tf_op jit(solution)/shard_map/gather | solution.py:168
  402.7 4.2 reshape.478
  406.9 3.8 fusion.76
  410.7 3.3 fusion.19
  (77 shorter events, 2.2 us)
Async XLA Ops:
  6.5 281.3 %copy-start = (bf16[1,256,2048]{2,1,0:T(8,128)(2,1)S(1)}, bf16[1,256,2048]{2,1,0:T(8,128)(2,1)}, u32[]{:S(2)}) copy-start(bf16[1,256,2048]{2,1,0:T(8,128)(2,1)} %param.30) | copy-start | bytes 3145732
  6.5 7.9 %copy-start.9 = (f32[128]{0:T(128)S(1)}, f32[128]{0:T(128)}, u32[]{:S(2)}) copy-start(f32[128]{0:T(128)} %param.23) | copy-start | bytes 1540
  6.5 45.6 %all-gather.6.cloned.1.call-start = ((), (), s32[]{:S(2)}) async-start(), calls=%async_computation.4 | async-start | bytes 1179648 | tf_op jit(solution)/shard_map/all_gather | solution.py:95
  9.7 83.8 %all-gather.4.cloned.1.call-start = ((), (), s32[]{:S(2)}) async-start(), calls=%async_computation.3 | async-start | bytes 1179648 | tf_op jit(solution)/shard_map/all_gather | solution.py:96
  15.2 3.5 copy-start.7
  97.2 3.4 copy-start.1
  106.4 3.4 copy-start.1
  115.6 3.4 copy-start.1
  124.8 3.4 copy-start.1
  134.0 3.4 copy-start.1
  143.3 3.4 copy-start.1
  152.5 3.4 copy-start.1
  161.7 3.4 copy-start.1
  167.3 14.3 %copy-start.5 = (bf16[128,2048]{1,0:T(8,128)(2,1)S(1)}, bf16[128,2048]{1,0:T(8,128)(2,1)}, u32[]{:S(2)}) copy-start(bf16[128,2048]{1,0:T(8,128)(2,1)} %param.21) | copy-start | bytes 1572868
  169.1 12.3 %all-to-all-start = ((bf16[4,128,512]{2,1,0:T(8,128)(2,1)}), bf16[4,128,512]{2,1,0:T(8,128)(2,1)S(1)}, u32[]{:S(2)}, u32[]{:S(2)}) async-start(bf16[4,128,512]{2,1,0:T(8,128)(2,1)} %all_to_all.20), calls=%async_computation | async-start | bytes 1048576 | tf_op jit(solution)/shard_map/all_to_all | solution.py:125
  181.6 4.8 %copy-start.6 = (f32[2048]{0:T(1024)S(1)}, f32[2048]{0:T(1024)}, u32[]{:S(2)}) copy-start(f32[2048]{0:T(1024)} %param.25) | copy-start | bytes 24580
  187.7 97.8 %copy-start.10 = (bf16[1,2048,256]{2,1,0:T(8,128)(2,1)S(1)}, bf16[1,2048,256]{2,1,0:T(8,128)(2,1)}, u32[]{:S(2)}) copy-start(bf16[1,2048,256]{2,1,0:T(8,128)(2,1)} %param.28) | copy-start | bytes 3145732
  283.6 2.0 copy-start.2
  297.0 4.1 copy-start.8
  297.0 4.3 %copy-start.4 = (bf16[2048,256]{1,0:T(8,128)(2,1)S(1)}, bf16[2048,256]{1,0:T(8,128)(2,1)}, u32[]{:S(2)}) copy-start(bf16[2048,256]{1,0:T(8,128)(2,1)} %param.31) | copy-start | bytes 3145732
  297.0 97.7 %all-to-all-start.2 = ((bf16[32,32,2048]{2,1,0:T(8,128)(2,1)}), bf16[32,32,2048]{2,1,0:T(8,128)(2,1)}, u32[]{:S(2)}, u32[]{:S(2)}) async-start(bf16[32,32,2048]{2,1,0:T(8,128)(2,1)} %convolution_convert_fusion), calls=%async_computation.2 | async-start | bytes 8388608 | tf_op jit(solution)/shard_map/all_to_all | solution.py:165
  402.7 8.0 %copy-start.3 = (bf16[256,2048]{1,0:T(8,128)(2,1)S(1)}, bf16[256,2048]{1,0:T(8,128)(2,1)}, u32[]{:S(2)}) copy-start(bf16[256,2048]{1,0:T(8,128)(2,1)} %param.33) | copy-start | bytes 3145732
Sparse Core Ops, SparseCore 0:
  9.9 42.2 all-gather.5
  54.2 39.2 all-gather.3
where the time goes:
time: 422 us; the launch traced here: 421 us
  waiting for transfers between devices  176 us (42%)
  blocking collectives  95.8 us (23%)
  matrix products  71 us (17%)
  other arithmetic  34.1 us (8%)
  local copies, waits for them, and re-layouts  21.8 us (5%)
  between operations  13.7 us (3%)
  starting transfers between devices  7.71 us (2%)
    all_to_all x1, blocking collectives, body(): lax.all_to_all(send_rows, ('sp', 'tp'), split_axis=0, concat_axis=0, tile...  95.8 us
    all_to_all x1, waiting for transfers between devices, body(): lax.all_to_all(processed, ('sp', 'tp'), split_axis=0, concat_axis=0, tile...  93 us
    all_gather x1, waiting for transfers between devices, body(): value_piece = lax.all_gather(values, 'sp', axis=0, tiled=True)  41.4 us
    all_gather x1, waiting for transfers between devices, body(): key_piece = lax.all_gather(k_rot, 'sp', axis=0, tiled=True)  32.9 us
    dot_general x8, matrix products, one_block(): jnp.einsum('gqd,kgd->gqk', query_3d, key_3d, preferred_element_type=jnp.f...  28.8 us
    reduce_sum x8, other arithmetic, one_block(): new_sum = running_sum * factor + jnp.sum(weights, axis=-1)  24.4 us
    dot_general x8, matrix products, one_block(): jnp.einsum('gqk,kgd->gqd', weights.astype(jnp.bfloat16), value_3d, prefer...  17.1 us
    dot_general x1, matrix products, expert_apply(): jnp.einsum('secf,efh->sech', hidden_e, expert_down, preferred_element_typ...  9.08 us
  transfers between devices with their start and end apart: 4, of which 4 were waited for; matrix products, arithmetic and copies ran while one was open for 2% of the time, Pallas kernels for 0%

commit v1 on v0

v1 whole, which is shorter than its diff:
```python
import functools
import math

import jax
import jax.numpy as jnp
from jax import lax
from jax.experimental import pallas as pl
from jax.experimental.pallas import tpu as pltpu
from jax.sharding import PartitionSpec as P

GRID_W = 64
MESH = pl.DeviceIdType.MESH


EPS = 1e-06
THETA = 10000.0


def norm_rotate(block, gain, cosine, sine):
    mean = jnp.mean(block * block, axis=-1, keepdims=True)
    block = block * lax.rsqrt(mean + EPS) * gain
    quarter = block.shape[-1] // 4
    lane = lax.broadcasted_iota(jnp.int32, block.shape, 1)
    after = pltpu.roll(block, 3 * quarter, 1)
    before = pltpu.roll(block, quarter, 1)
    partner = jnp.where((lane // quarter) % 2 == 0, after, before)
    return (block * cosine + partner * sine).astype(jnp.bfloat16)


def plane_peer(z, d, planes):
    if planes == 4:
        return (z + 1 - 2 * (z % 2), z + 2 - 4 * (z // 2), 3 - z)[d - 1]
    return planes - 1 - z


def attention_kernel(
    n_sp, n_tp, planes, group,
    q_ref, k_ref, v_ref, cos_ref, sin_ref, qg_ref, kg_ref, out_ref,
    held, q_rot, top, total, accum, rows_out,
    send_z, send_y, recv_kv, send_o, recv_o,
):
    per = n_sp // planes
    me_sp = lax.axis_index("sp")
    me_tp = lax.axis_index("tp")
    z, y = me_sp // per, me_sp % per
    tok, width = k_ref.shape
    piece = tok // n_tp
    lanes = group * width
    held[me_sp, 0] = norm_rotate(
        k_ref[...].astype(jnp.float32), kg_ref[...], cos_ref[...], sin_ref[...]
    )
    held[me_sp, 1] = v_ref[...]
    barrier = pltpu.get_barrier_semaphore()
    for d in range(1, n_sp):
        pl.semaphore_signal(
            barrier, inc=1, device_id={"sp": lax.rem(me_sp + d, n_sp)}, device_id_type=MESH
        )
    for d in range(1, n_tp):
        pl.semaphore_signal(
            barrier, inc=1, device_id={"tp": lax.rem(me_tp + d, n_tp)}, device_id_type=MESH
        )
    pl.semaphore_wait(barrier, n_sp + n_tp - 2)

    def block_copy(block, target, sem):
        return pltpu.make_async_remote_copy(
            src_ref=held.at[block], dst_ref=held.at[block],
            send_sem=sem, recv_sem=recv_kv.at[block],
            device_id={"sp": target}, device_id_type=MESH,
        )

    def to_plane(slot, block):
        for d in range(1, per):
            block_copy(block, z * per + lax.rem(y + d, per), send_y.at[slot, d - 1]).start()

    for d in range(1, planes):
        if d == 1:
            block_copy(me_sp, plane_peer(z, d, planes) * per + y, send_z.at[d - 1]).start()
            to_plane(0, me_sp)
        else:
            block_copy(me_sp, plane_peer(z, d, planes) * per + y, send_z.at[d - 1]).start()
    for j in range(n_tp):
        rows = pl.ds(j * piece, piece)
        for h in range(group):
            q_rot[j, pl.ds(h * piece, piece), :] = norm_rotate(
                q_ref[rows, pl.ds(h * width, width)].astype(jnp.float32),
                qg_ref[...], cos_ref[rows, :], sin_ref[rows, :],
            )
    top[...] = jnp.full(top.shape, -1e30, jnp.float32)
    total[...] = jnp.zeros(total.shape, jnp.float32)
    accum[...] = jnp.zeros(accum.shape, jnp.float32)
    factor = math.log2(math.e) / math.sqrt(width)
    repeat = tok // width

    def attend(block, j):
        scores = lax.dot_general(
            q_rot[j], held[block, 0], (((1,), (1,)), ((), ())),
            preferred_element_type=jnp.float32,
        )
        old = top[j]
        new = jnp.maximum(old, jnp.max(scores, axis=1, keepdims=True))
        weights = jnp.exp2((scores - jnp.concatenate([new] * repeat, axis=1)) * factor)
        alpha = jnp.exp2((old - new) * factor)
        part = weights[:, :width]
        for r in range(1, repeat):
            part = part + weights[:, r * width:(r + 1) * width]
        summed = total[j] * alpha + part
        added = jnp.dot(
            weights.astype(jnp.bfloat16), held[block, 1], preferred_element_type=jnp.float32
        )
        return new, summed, accum[j] * alpha + added

    def out_copy(j):
        return pltpu.make_async_remote_copy(
            src_ref=rows_out.at[j],
            dst_ref=out_ref.at[:, pl.ds(pl.multiple_of(me_tp * lanes, 128), lanes)],
            send_sem=send_o.at[j], recv_sem=recv_o.at[me_tp],
            device_id={"tp": j}, device_id_type=MESH,
        )

    def step(block):
        @pl.loop(0, n_tp)
        def _(j):
            new, summed, acc = attend(block, j)
            top[j] = new
            total[j] = summed
            accum[j] = acc

    def arrive(block):
        block_copy(block, me_sp, send_z.at[0]).wait_recv()

    def others(plane, finish=False):
        for d in range(1, per):
            block = plane * per + lax.rem(y + d, per)
            arrive(block)
            step(block)

    step(me_sp)
    previous = z
    for d in range(1, planes):
        plane = plane_peer(z, d, planes)
        block = plane * per + y
        arrive(block)
        to_plane(d, block)
        others(previous)
        step(block)
        previous = plane
    others(previous)

    for d in range(n_tp):
        j = lax.rem(me_tp + 1 + d, n_tp)
        result = accum[j] / jnp.sum(total[j], axis=1, keepdims=True)
        result = result.astype(jnp.bfloat16)
        for h in range(group):
            rows_out[j, :, pl.ds(h * width, width)] = result[h * piece:(h + 1) * piece]
        if d < n_tp - 1:
            out_copy(j).start()
        else:
            for h in range(group):
                out_ref[:, pl.ds(pl.multiple_of(me_tp * lanes + h * width, 128), width)] = result[
                    h * piece:(h + 1) * piece
                ]
    for d in range(1, n_tp):
        source = lax.rem(me_tp + d, n_tp)
        pltpu.make_async_remote_copy(
            src_ref=rows_out.at[source],
            dst_ref=out_ref.at[:, pl.ds(pl.multiple_of(source * lanes, 128), lanes)],
            send_sem=send_o.at[source], recv_sem=recv_o.at[source],
            device_id={"tp": source}, device_id_type=MESH,
        ).wait()
    for d in range(1, planes):
        block_copy(me_sp, me_sp, send_z.at[d - 1]).wait_send()
    for slot in range(planes):
        for d in range(1, per):
            block_copy(me_sp, me_sp, send_y.at[slot, d - 1]).wait_send()


def attention(mesh_sp, mesh_tp, queries, keys, values, query_gain, key_gain):
    tok, width = keys.shape
    group = queries.shape[1] // width
    planes = 4 if mesh_sp % 4 == 0 else 2
    per = mesh_sp // planes
    piece = tok // mesh_tp
    quarter = width // 4
    inverse = jnp.power(THETA, -4.0 * jnp.arange(quarter, dtype=jnp.float32) / width)
    start = lax.axis_index("sp") * tok
    grid_rows = tok // GRID_W
    row_angle = (start // GRID_W + jnp.arange(grid_rows)).astype(jnp.float32)[:, None] * inverse
    col_angle = jnp.arange(GRID_W).astype(jnp.float32)[:, None] * inverse

    def spread(row_part, col_part, sign):
        row_part = jnp.broadcast_to(row_part[:, None, :], (grid_rows, GRID_W, quarter))
        col_part = jnp.broadcast_to(col_part[None, :, :], (grid_rows, GRID_W, quarter))
        return jnp.concatenate(
            [sign * row_part, row_part, sign * col_part, col_part], axis=-1
        ).reshape(tok, width)

    tables = lax.optimization_barrier(
        (jnp.cos(row_angle), jnp.cos(col_angle), jnp.sin(row_angle), jnp.sin(col_angle))
    )
    cosine = spread(tables[0], tables[1], 1.0)
    sine = spread(tables[2], tables[3], -1.0)
    vmem = pl.BlockSpec(memory_space=pltpu.VMEM)
    return pl.pallas_call(
        functools.partial(attention_kernel, mesh_sp, mesh_tp, planes, group),
        out_shape=jax.ShapeDtypeStruct((piece, mesh_tp * group * width), jnp.bfloat16),
        in_specs=[vmem] * 7,
        out_specs=vmem,
        scratch_shapes=[
            pltpu.VMEM((mesh_sp, 2, tok, width), jnp.bfloat16),
            pltpu.VMEM((mesh_tp, group * piece, width), jnp.bfloat16),
            pltpu.VMEM((mesh_tp, group * piece, width), jnp.float32),
            pltpu.VMEM((mesh_tp, group * piece, width), jnp.float32),
            pltpu.VMEM((mesh_tp, group * piece, width), jnp.float32),
            pltpu.VMEM((mesh_tp, piece, group * width), jnp.bfloat16),
            pltpu.SemaphoreType.DMA((planes - 1,)),
            pltpu.SemaphoreType.DMA((planes, max(per - 1, 1))),
            pltpu.SemaphoreType.DMA((mesh_sp,)),
            pltpu.SemaphoreType.DMA((mesh_tp,)),
            pltpu.SemaphoreType.DMA((mesh_tp,)),
        ],
        compiler_params=pltpu.CompilerParams(
            collective_id=0, has_side_effects=True, vmem_limit_bytes=48 * 2**20
        ),
        name="attention",
    )(queries, keys, values, cosine, sine, query_gain.reshape(1, width), key_gain.reshape(1, width))


def expert_apply(arrived, expert_gate, expert_up, expert_down):
    sources, slots, width = arrived.shape
    local = expert_gate.shape[0]
    grouped = arrived.reshape(sources // local, local, slots, width)
    gate_part = jnp.einsum(
        "sech,ehf->secf", grouped, expert_gate, preferred_element_type=jnp.float32
    )
    up_part = jnp.einsum("sech,ehf->secf", grouped, expert_up, preferred_element_type=jnp.float32)
    hidden_e = (jax.nn.silu(gate_part) * up_part).astype(jnp.bfloat16)
    result = jnp.einsum("secf,efh->sech", hidden_e, expert_down, preferred_element_type=jnp.float32)
    return result.astype(jnp.bfloat16).reshape(sources, slots, width)


def body(
    queries,
    keys,
    values,
    residual,
    out_proj,
    query_gain,
    key_gain,
    norm_gain,
    routes,
    route_weight,
    expert_gate,
    expert_up,
    expert_down,
    shared_gate,
    shared_up,
    shared_down,
):
    all_heads = attention(
        lax.axis_size("sp"), lax.axis_size("tp"), queries, keys, values, query_gain, key_gain
    )
    projected = jnp.dot(all_heads, out_proj, preferred_element_type=jnp.float32)
    hidden1 = (residual.astype(jnp.float32) + projected).astype(jnp.bfloat16)
    hidden_f = hidden1.astype(jnp.float32)
    normed = (
        hidden_f
        * lax.rsqrt(jnp.mean(hidden_f * hidden_f, axis=-1, keepdims=True) + EPS)
        * norm_gain
    ).astype(jnp.bfloat16)
    rows_local = normed.shape[0]
    top_count = routes.shape[1]
    pair_count = rows_local * top_count
    expert_total = expert_gate.shape[0] * lax.axis_size("sp") * lax.axis_size("tp")
    capacity = max(2, 2 * rows_local * top_count // expert_total)
    flat_routes = routes.reshape(pair_count)
    one_hot = (flat_routes[:, None] == jnp.arange(expert_total, dtype=jnp.int32)[None, :]).astype(
        jnp.float32
    )
    lower = (jnp.arange(pair_count)[:, None] >= jnp.arange(pair_count)[None, :]).astype(jnp.float32)
    running_count = jnp.dot(lower, one_hot, precision=lax.Precision.HIGHEST)
    slot_place = (jnp.sum(running_count * one_hot, axis=1) - 1.0).astype(jnp.int32)
    slot_index = flat_routes * capacity + slot_place
    slot_total = expert_total * capacity
    chosen = jnp.arange(slot_total, dtype=jnp.int32)[None, :, None] == slot_index.reshape(
        rows_local, 1, top_count
    )
    placement = jnp.any(chosen, axis=2).astype(jnp.bfloat16)
    weighted = jnp.sum(jnp.where(chosen, route_weight[:, None, :], 0.0), axis=2)
    send_rows = lax.dot_general(
        placement, normed, (((0,), (0,)), ((), ())), preferred_element_type=jnp.float32
    ).astype(jnp.bfloat16)
    send_rows = send_rows.reshape(expert_total, capacity, normed.shape[1])
    shared_hidden = (
        jax.nn.silu(jnp.dot(normed, shared_gate, preferred_element_type=jnp.float32))
        * jnp.dot(normed, shared_up, preferred_element_type=jnp.float32)
    ).astype(jnp.bfloat16)
    shared_out = jnp.dot(shared_hidden, shared_down, preferred_element_type=jnp.float32)
    processed = expert_apply(
        lax.all_to_all(send_rows, ("sp", "tp"), split_axis=0, concat_axis=0, tiled=True),
        expert_gate,
        expert_up,
        expert_down,
    )
    returned = lax.all_to_all(processed, ("sp", "tp"), split_axis=0, concat_axis=0, tiled=True)
    returned = returned.reshape(slot_total, normed.shape[1])
    mixed = shared_out + jnp.dot(
        weighted.astype(jnp.bfloat16), returned, preferred_element_type=jnp.float32
    )
    return (hidden_f + mixed).astype(jnp.bfloat16)


def solution(mesh):
    placed = (
        P("sp", "tp"),
        P("sp", "tp"),
        P("sp", "tp"),
        P(("sp", "tp"), None),
        P(),
        P(),
        P(),
        P(),
        P(("sp", "tp"), None),
        P(("sp", "tp"), None),
        P(("sp", "tp"), None, None),
        P(("sp", "tp"), None, None),
        P(("sp", "tp"), None, None),
        P(),
        P(),
        P(),
    )
    return jax.shard_map(
        body, mesh=mesh, in_specs=placed, out_specs=P(("sp", "tp"), None), check_vma=False
    )
```

time: 422 us -> 269 us (0.64)
  waiting for transfers between devices: 176 us -> 88.5 us
  Pallas kernels: 0 us -> 44.7 us
  matrix products: 71 us -> 26.6 us
  other arithmetic: 34.1 us -> 1.74 us
  local copies, waits for them, and re-layouts: 21.8 us -> 5.66 us
  between operations: 13.7 us -> 0.25 us
    all_gather x2 -> x0, waiting for transfers between devices: 74.4 us -> none  [the longest x1 41.4 us: body(): value_piece = lax.all_gather(values, 'sp', axis=0, tiled=True)]
    dot_general x18 -> x2, matrix products: 51 us -> 5.33 us  [the longest x1 4.03 us: body(): jnp.dot(weighted.astype(jnp.bfloat16), returned, preferred_element_type=j...]
    pallas_call x0 -> x1, Pallas kernels: none -> 44.7 us  [attention(): pl.pallas_call(functools.partial(attention_kernel, mesh_sp, mesh_tp, plan...]
    reduce_sum x11 -> x1, other arithmetic: 25.3 us -> 0.29 us  [body(): weighted = jnp.sum(jnp.where(chosen, route_weight[:, None, :], 0.0), axis=2)]
    all_to_all x1 -> x0, waiting for transfers between devices: 8.13 us -> none  [body(): lax.all_to_all(attn_local, 'tp', split_axis=0, concat_axis=1, tiled=True)]
    gather x1 -> x0, local copies, waits for them, and re-layouts: 8 us -> none  [body(): returned[slot_index].reshape(rows_local, top_count, normed.shape[1])]
    reshape x3 -> x0, local copies, waits for them, and re-layouts: 5.97 us -> none  [the longest x1 4.19 us: body(): returned[slot_index].reshape(rows_local, top_count, normed.shape[1])]
    all_to_all x1, waiting for transfers between devices: 93 us -> 88.5 us  [body(): lax.all_to_all(processed, ('sp', 'tp'), split_axis=0, concat_axis=0, tile...]
  transfers between devices with their start and end apart: 4 -> 1, of which waited for: 4 -> 1; matrix products, arithmetic and copies ran while one was open for 2% -> 2% of each run, Pallas kernels for 0% -> 0%
where the time goes in v1:
time: 269 us; the launch traced here: 268 us
  blocking collectives  97.2 us (36%)
  waiting for transfers between devices  88.5 us (33%)
  Pallas kernels  44.7 us (17%)
  matrix products  26.6 us (10%)
  local copies, waits for them, and re-layouts  5.66 us (2%)
  starting transfers between devices  3.79 us (1%)
    all_to_all x1, blocking collectives, body(): lax.all_to_all(send_rows, ('sp', 'tp'), split_axis=0, concat_axis=0, tile...  97.2 us
    all_to_all x1, waiting for transfers between devices, body(): lax.all_to_all(processed, ('sp', 'tp'), split_axis=0, concat_axis=0, tile...  88.5 us
    pallas_call x1, Pallas kernels, attention(): pl.pallas_call(functools.partial(attention_kernel, mesh_sp, mesh_tp, plan...  44.7 us
    dot_general x1, matrix products, expert_apply(): jnp.einsum('secf,efh->sech', hidden_e, expert_down, preferred_element_typ...  9.06 us
  transfers between devices with their start and end apart: 1, of which 1 were waited for; matrix products, arithmetic and copies ran while one was open for 2% of the time, Pallas kernels for 0%

profile of v1, /device:TPU:0, one launch (start us, length us, event | category | flops | bytes accessed | tf_op | source)
XLA Modules:
  0.0 268.4 jit_solution(130675981811433546)
XLA Ops:
  0.0 0.0 copy-start
  0.0 0.0 copy-start.1
  0.0 0.0 copy-start.7
  0.1 0.1 multiply_sine_fusion.1
  0.2 0.2 multiply_sine_fusion
  0.4 0.3 pad_maximum_fusion
  0.8 0.3 pad_maximum_fusion.1
  1.1 0.0 copy-done.1
  1.1 0.0 copy-start.2
  1.1 0.9 copy-done.2
  2.0 0.0 copy-start.3
  2.0 0.9 copy-done.3
  2.9 0.0 copy-start.4
  2.9 0.7 copy-done.4
  3.6 0.0 copy-start.5
  3.6 0.7 copy-done.5
  4.3 44.7 %attention.1 = bf16[128,2048]{1,0:T(8,128)(2,1)S(1)} custom-call(bf16[512,512]{1,0:T(8,128)(2,1)S(1)} %copy-done.1, bf16[512,128]{1,0:T(8,128)(2,1)S(1)} %copy-done.2, bf16[512,128]{1,0:T(8,128)(2,1)S(1)} %copy-done.3, f32[512,128]{1,0:T(8,128)S(1)} %bitcast.56, f32[512,128]{1,0:T(8,128)S(1)} %bitcast.57, f32[1,128]{1,0:T(1,128)S(1)} %bitcast.58, ...), custom_call_target="tpu_custom_call" | custom-call | tf_op jit(solution)/shard_map/attention/pallas_call | solution.py:203
  48.9 0.0 copy-done.7
  48.9 0.0 copy-start.9
  49.0 0.0 copy-start.8
  49.0 4.8 %multiply_reduce_fusion = (f32[128]{0:T(128)S(1)}, f32[128,2048]{1,0:T(8,128)S(1)}) fusion(bf16[128,2048]{1,0:T(8,128)(2,1)S(1)} %attention.1, bf16[2048,2048]{1,0:T(8,128)(2,1)} %param.20, bf16[128,2048]{1,0:T(8,128)(2,1)S(1)} %copy-done.7), kind=kOutput, calls=%fused_computation.31 | convolution fusion | flops 1075314560 | bytes 10486272 | tf_op jit(solution)/shard_map/dot_general | solution.py:262
  53.8 0.0 copy-done.9
  53.8 0.1 copy.27
  53.9 0.1 eq.29
  54.0 0.3 fusion.10
  54.3 0.1 convert_element_type.68
  54.4 0.1 copy.28
  54.5 0.4 fusion.4
  54.9 0.0 copy-done.8
  54.9 0.2 multiply_convert_fusion
  55.0 1.3 convolution_convert_fusion.1
  56.3 0.0 copy-start.11
  56.4 97.2 %all_to_all.10 = bf16[32,32,2048]{2,1,0:T(8,128)(2,1)S(1)} all-to-all(bf16[32,32,2048]{2,1,0:T(8,128)(2,1)S(1)} %bitcast.60), channel_id=1, replica_groups=mesh['sp'=8,'tp'=4] {'sp','tp'}, dimensions={0} | all-to-all | bytes 8388608 | tf_op jit(solution)/shard_map/all_to_all | solution.py:299
  153.6 0.0 copy-start.6
  153.6 2.0 copy-done.6
  155.5 0.0 copy-done.11
  155.5 2.3 convolution_bitcast_fusion.1
  157.8 0.0 copy-done
  157.8 9.1 %convolution_convert_fusion = bf16[32,32,2048]{2,1,0:T(8,128)(2,1)} fusion(bf16[32,32,2048]{2,1,0:T(8,128)(2,1)} %copy-done.6, bf16[1,256,2048]{2,1,0:T(8,128)(2,1)S(1)} %copy-done, bf16[1,2048,256]{2,1,0:T(8,128)(2,1)} %param.27, f32[32,1,32,256]{3,2,0,1:T(8,128)} %convolution_bitcast_fusion.1), kind=kOutput, calls=%fused_computation | convolution fusion | flops 2151153664 | bytes 11534336 | tf_op jit(solution)/shard_map/secf,efh->sech/dot_general | solution.py:237
  166.9 0.0 copy-start.10
  166.9 3.8 %all-to-all-start.1 = ((bf16[32,32,2048]{2,1,0:T(8,128)(2,1)}), bf16[32,32,2048]{2,1,0:T(8,128)(2,1)}, u32[]{:S(2)}, u32[]{:S(2)}) async-start(bf16[32,32,2048]{2,1,0:T(8,128)(2,1)} %convolution_convert_fusion), calls=%async_computation.1 | async-start | bytes 8388608 | tf_op jit(solution)/shard_map/all_to_all | solution.py:304
  170.7 0.0 copy-done.10
  170.7 0.3 select_reduce_fusion
  171.0 1.5 fusion.31
  172.5 3.4 %fusion.9 = f32[128,2048]{1,0:T(8,128)} fusion(bf16[256,2048]{1,0:T(8,128)(2,1)} %param.31, bf16[128,2048]{1,0:T(8,128)(2,1)S(1)} %multiply_convert_fusion, bf16[2048,256]{1,0:T(8,128)(2,1)} %param.30, f32[128,256]{1,0:T(8,128)S(1)} %fusion.31), kind=kOutput, calls=%fused_computation.19 | convolution fusion | flops 268632064 | bytes 3801088 | tf_op jit(solution)/shard_map/dot_general | solution.py:297
  175.9 88.5 %all-to-all-done.1 = bf16[32,32,2048]{2,1,0:T(8,128)(2,1)} async-done(((bf16[32,32,2048]{2,1,0:T(8,128)(2,1)}), bf16[32,32,2048]{2,1,0:T(8,128)(2,1)}, u32[]{:S(2)}, u32[]{:S(2)}) %all-to-all-start.1) | async-done | bytes 4194336 | tf_op jit(solution)/shard_map/all_to_all | solution.py:304
  264.4 4.0 %fusion.3 = bf16[128,2048]{1,0:T(8,128)(2,1)} fusion(f32[128,2048]{1,0:T(8,128)S(1)} %get-tuple-element.18, f32[128,2048]{1,0:T(8,128)} %fusion.9, bf16[1024,2048]{1,0:T(8,128)(2,1)} %bitcast.20, bf16[128,1024]{1,0:T(8,128)(2,1)S(1)} %select_reduce_fusion), kind=kOutput, calls=%fused_computation.7 | convolution fusion | flops 537657344 | bytes 7077888 | tf_op jit(solution)/shard_map/dot_general | solution.py:306
  (14 shorter events, 0.2 us)
Async XLA Ops:
  0.0 157.8 %copy-start = (bf16[1,256,2048]{2,1,0:T(8,128)(2,1)S(1)}, bf16[1,256,2048]{2,1,0:T(8,128)(2,1)}, u32[]{:S(2)}) copy-start(bf16[1,256,2048]{2,1,0:T(8,128)(2,1)} %param.28) | copy-start | bytes 3145732
  0.0 1.1 copy-start.1
  0.0 48.9 %copy-start.7 = (bf16[128,2048]{1,0:T(8,128)(2,1)S(1)}, bf16[128,2048]{1,0:T(8,128)(2,1)}, u32[]{:S(2)}) copy-start(bf16[128,2048]{1,0:T(8,128)(2,1)} %param.19) | copy-start | bytes 1572868
  1.1 0.9 copy-start.2
  2.0 0.9 copy-start.3
  2.9 0.7 copy-start.4
  3.6 0.7 copy-start.5
  48.9 4.8 %copy-start.9 = (s32[128,4]{0,1:T(4,128)S(1)}, s32[128,4]{0,1:T(4,128)}, u32[]{:S(2)}) copy-start(s32[128,4]{0,1:T(4,128)} %param.24) | copy-start | bytes 6148
  49.0 5.9 %copy-start.8 = (f32[2048]{0:T(1024)S(1)}, f32[2048]{0:T(1024)}, u32[]{:S(2)}) copy-start(f32[2048]{0:T(1024)} %param.23) | copy-start | bytes 24580
  56.3 99.2 %copy-start.11 = (bf16[1,2048,256]{2,1,0:T(8,128)(2,1)S(1)}, bf16[1,2048,256]{2,1,0:T(8,128)(2,1)}, u32[]{:S(2)}) copy-start(bf16[1,2048,256]{2,1,0:T(8,128)(2,1)} %param.26) | copy-start | bytes 3145732
  153.6 2.0 copy-start.6
  166.9 3.8 %copy-start.10 = (f32[128,4]{0,1:T(4,128)S(1)}, f32[128,4]{0,1:T(4,128)}, u32[]{:S(2)}) copy-start(f32[128,4]{0,1:T(4,128)} %param.25) | copy-start | bytes 6148
  166.9 97.5 %all-to-all-start.1 = ((bf16[32,32,2048]{2,1,0:T(8,128)(2,1)}), bf16[32,32,2048]{2,1,0:T(8,128)(2,1)}, u32[]{:S(2)}, u32[]{:S(2)}) async-start(bf16[32,32,2048]{2,1,0:T(8,128)(2,1)} %convolution_convert_fusion), calls=%async_computation.1 | async-start | bytes 8388608 | tf_op jit(solution)/shard_map/all_to_all | solution.py:304

commit v2 on v1

--- a/solution.py
+++ b/solution.py
@@ -219,23 +219,253 @@
             pltpu.SemaphoreType.DMA((mesh_tp,)),
         ],
         compiler_params=pltpu.CompilerParams(
-            collective_id=0, has_side_effects=True, vmem_limit_bytes=48 * 2**20
+            collective_id=0, has_side_effects=True, vmem_limit_bytes=40 * 2**20
         ),
         name="attention",
     )(queries, keys, values, cosine, sine, query_gain.reshape(1, width), key_gain.reshape(1, width))
 
 
-def expert_apply(arrived, expert_gate, expert_up, expert_down):
-    sources, slots, width = arrived.shape
-    local = expert_gate.shape[0]
-    grouped = arrived.reshape(sources // local, local, slots, width)
-    gate_part = jnp.einsum(
-        "sech,ehf->secf", grouped, expert_gate, preferred_element_type=jnp.float32
-    )
-    up_part = jnp.einsum("sech,ehf->secf", grouped, expert_up, preferred_element_type=jnp.float32)
-    hidden_e = (jax.nn.silu(gate_part) * up_part).astype(jnp.bfloat16)
-    result = jnp.einsum("secf,efh->sech", hidden_e, expert_down, preferred_element_type=jnp.float32)
-    return result.astype(jnp.bfloat16).reshape(sources, slots, width)
+def expert_kernel(
+    n_sp, n_tp, planes, cap, top_count, chunks,
+    info_ref, normed_ref, hidden_ref, gate_ref, up_ref, down_ref,
+    sgate_ref, sup_ref, sdown_ref, out_ref,
+    info, gathered, sent, arrived, answers, returned, partial, sums,
+    place, combine, acc, hid,
+    s_info, r_info, s_z, r_z, s_in, r_in, s_back, r_back, s_sum, r_sum,
+):
+    per = n_sp // planes
+    team = per * n_tp
+    me_sp = lax.axis_index("sp")
+    me_tp = lax.axis_index("tp")
+    z, y = me_sp // per, me_sp % per
+    me = y * n_tp + me_tp
+    rows = normed_ref.shape[0]
+    wide = normed_ref.shape[1] // chunks
+    share = planes * cap
+    slots = team * share
+    tile = math.gcd(slots, 256)
+
+    def in_plane(p):
+        return {"sp": z * per + p // n_tp, "tp": p % n_tp}
+
+    def at_plane(d):
+        return {"sp": plane_peer(z, d, planes) * per + y}
+
+    def block(p, size):
+        return pl.ds(pl.multiple_of(p * size, size), size)
+
+    def remote(src, dst, send, recv, target):
+        return pltpu.make_async_remote_copy(
+            src_ref=src, dst_ref=dst, send_sem=send, recv_sem=recv,
+            device_id=target, device_id_type=MESH,
+        )
+
+    def cols(c):
+        return pl.ds(c * wide, wide)
+
+    barrier = pltpu.get_barrier_semaphore()
+
+    @pl.loop(1, team)
+    def _(d):
+        pl.semaphore_signal(
+            barrier, inc=1, device_id=in_plane(lax.rem(me + d, team)), device_id_type=MESH
+        )
+
+    for d in range(1, planes):
+        pl.semaphore_signal(barrier, inc=1, device_id=at_plane(d), device_id_type=MESH)
+    pl.semaphore_wait(barrier, team + planes - 2)
+
+    def info_copy(d, source):
+        return remote(info_ref, info.at[source], s_info.at[d], r_info.at[source], at_plane(d))
+
+    def z_copy(c, d, source):
+        return remote(
+            normed_ref.at[:, cols(c)], gathered.at[c, block(source, rows)],
+            s_z.at[c, d], r_z.at[c, source], at_plane(d),
+        )
+
+    def in_copy(c, p, source):
+        return remote(
+            sent.at[c, block(p, share)], arrived.at[c, block(source, share)],
+            s_in.at[c, p], r_in.at[c, source], in_plane(p),
+        )
+
+    def back_copy(c, p, source):
+        return remote(
+            answers.at[c, block(p, share)], returned.at[c, block(source, share)],
+            s_back.at[c, p], r_back.at[c, source], in_plane(p),
+        )
+
+    def sum_copy(c, d, source):
+        return remote(
+            partial.at[c, block(plane_peer(z, d, planes), rows)], sums.at[c, source],
+            s_sum.at[c, d], r_sum.at[c, source], at_plane(d),
+        )
+
+    for d in range(1, planes):
+        info_copy(d, z).start()
+    for c in range(chunks):
+        for d in range(1, planes):
+            z_copy(c, d, z).start()
+        gathered[c, block(z, rows)] = normed_ref[:, cols(c)]
+    info[z] = info_ref[...]
+
+    shared_gate = jnp.dot(normed_ref[...], sgate_ref[...], preferred_element_type=jnp.float32)
+    shared_up = jnp.dot(normed_ref[...], sup_ref[...], preferred_element_type=jnp.float32)
+    shared_hid = (jax.nn.silu(shared_gate) * shared_up).astype(jnp.bfloat16)
+    for c in range(chunks):
+        out_ref[:, cols(c)] = jnp.dot(
+            shared_hid, sdown_ref[:, cols(c)], preferred_element_type=jnp.float32
+        ) + hidden_ref[:, cols(c)].astype(jnp.float32)
+
+    number = lax.broadcasted_iota(jnp.int32, (slots, rows), 0)
+    owner = (number // cap) % planes
+    slot = ((z * team + number // share) * cap + number % cap).astype(jnp.float32)
+    for d in range(1, planes):
+        info_copy(d, plane_peer(z, d, planes)).wait_recv()
+    for plane in range(planes):
+        wanted = jnp.where(owner == plane, slot, -1.0)
+        ones = jnp.zeros((slots, rows), jnp.float32)
+        shares = jnp.zeros((slots, rows), jnp.float32)
+        for k in range(top_count):
+            match = wanted == info[plane, k:k + 1, :]
+            ones = jnp.where(match, 1.0, ones)
+            shares = jnp.where(match, info[plane, top_count + k:top_count + k + 1, :], shares)
+        place[:, pl.ds(plane * rows, rows)] = ones.astype(jnp.bfloat16)
+        combine[pl.ds(plane * rows, rows), :] = shares.T.astype(jnp.bfloat16)
+
+    for c in range(chunks):
+        for d in range(1, planes):
+            z_copy(c, d, plane_peer(z, d, planes)).wait_recv()
+
+        @pl.loop(0, slots // tile)
+        def _(i):
+            sent[c, block(i, tile)] = jnp.dot(
+                place[block(i, tile), :], gathered[c], preferred_element_type=jnp.float32
+            ).astype(jnp.bfloat16)
+
+        @pl.loop(1, team)
+        def _(d):
+            in_copy(c, lax.rem(me + d, team), me).start()
+
+        arrived[c, block(me, share)] = sent[c, block(me, share)]
+
+    inner = gate_ref.shape[2]
+    for c in range(chunks):
+        @pl.loop(1, team)
+        def _(d):
+            source = lax.rem(me + d, team)
+            in_copy(c, source, source).wait_recv()
+
+        @pl.loop(0, slots // tile)
+        def _(i):
+            part = arrived[c, block(i, tile)]
+            gate = jnp.dot(part, gate_ref[0, cols(c), :], preferred_element_type=jnp.float32)
+            up = jnp.dot(part, up_ref[0, cols(c), :], preferred_element_type=jnp.float32)
+            if c > 0:
+                gate = gate + acc[block(i, tile), pl.ds(0, inner)]
+                up = up + acc[block(i, tile), pl.ds(inner, inner)]
+            if c < chunks - 1:
+                acc[block(i, tile), pl.ds(0, inner)] = gate
+                acc[block(i, tile), pl.ds(inner, inner)] = up
+            else:
+                hid[block(i, tile), :] = (jax.nn.silu(gate) * up).astype(jnp.bfloat16)
+
+    for c in range(chunks):
+        @pl.loop(0, slots // tile)
+        def _(i):
+            answers[c, block(i, tile)] = jnp.dot(
+                hid[block(i, tile), :], down_ref[0, :, cols(c)],
+                preferred_element_type=jnp.float32,
+            ).astype(jnp.bfloat16)
+
+        @pl.loop(1, team)
+        def _(d):
+            back_copy(c, lax.rem(me + d, team), me).start()
+
+        returned[c, block(me, share)] = answers[c, block(me, share)]
+
+    for c in range(chunks):
+        @pl.loop(1, team)
+        def _(d):
+            source = lax.rem(me + d, team)
+            back_copy(c, source, source).wait_recv()
+
+        @pl.loop(0, planes)
+        def _(i):
+            partial[c, block(i, rows)] = jnp.dot(
+                combine[block(i, rows), :], returned[c], preferred_element_type=jnp.float32
+            ).astype(jnp.bfloat16)
+
+        for d in range(1, planes):
+            sum_copy(c, d, z).start()
+        sums[c, z] = partial[c, block(z, rows)]
+
+    for c in range(chunks):
+        for d in range(1, planes):
+            sum_copy(c, d, plane_peer(z, d, planes)).wait_recv()
+        result = out_ref[:, cols(c)]
+        for plane in range(planes):
+            result = result + sums[c, plane].astype(jnp.float32)
+        out_ref[:, cols(c)] = result
+
+    for d in range(1, planes):
+        info_copy(d, z).wait_send()
+    for c in range(chunks):
+        for d in range(1, planes):
+            z_copy(c, d, z).wait_send()
+            sum_copy(c, d, z).wait_send()
+
+        @pl.loop(1, team)
+        def _(d):
+            p = lax.rem(me + d, team)
+            in_copy(c, p, me).wait_send()
+            back_copy(c, p, me).wait_send()
+
+
+def routed_experts(
+    info, normed, hidden1, gate, up, down, shared_gate, shared_up, shared_down, cap
+):
+    n_sp, n_tp = lax.axis_size("sp"), lax.axis_size("tp")
+    rows, model = normed.shape
+    planes = 4 if n_sp % 4 == 0 else 2
+    team = n_sp // planes * n_tp
+    chunks = 4
+    wide = model // chunks
+    slots = team * planes * cap
+    inner = gate.shape[2]
+    top_count = info.shape[0] // 2
+    vmem = pl.BlockSpec(memory_space=pltpu.VMEM)
+    dma = pltpu.SemaphoreType.DMA
+    return pl.pallas_call(
+        functools.partial(expert_kernel, n_sp, n_tp, planes, cap, top_count, chunks),
+        out_shape=jax.ShapeDtypeStruct((rows, model), jnp.float32),
+        in_specs=[vmem] * 9,
+        out_specs=vmem,
+        scratch_shapes=[
+            pltpu.VMEM((planes,) + info.shape, jnp.float32),
+            pltpu.VMEM((chunks, planes * rows, wide), jnp.bfloat16),
+            pltpu.VMEM((chunks, slots, wide), jnp.bfloat16),
+            pltpu.VMEM((chunks, slots, wide), jnp.bfloat16),
+            pltpu.VMEM((chunks, slots, wide), jnp.bfloat16),
+            pltpu.VMEM((chunks, slots, wide), jnp.bfloat16),
+            pltpu.VMEM((chunks, planes * rows, wide), jnp.bfloat16),
+            pltpu.VMEM((chunks, planes, rows, wide), jnp.bfloat16),
+            pltpu.VMEM((slots, planes * rows), jnp.bfloat16),
+            pltpu.VMEM((planes * rows, slots), jnp.bfloat16),
+            pltpu.VMEM((slots, 2 * inner), jnp.float32),
+            pltpu.VMEM((slots, inner), jnp.bfloat16),
+            dma((planes,)), dma((planes,)),
+            dma((chunks, planes)), dma((chunks, planes)),
+            dma((chunks, team)), dma((chunks, team)),
+            dma((chunks, team)), dma((chunks, team)),
+            dma((chunks, planes)), dma((chunks, planes)),
+        ],
+        compiler_params=pltpu.CompilerParams(
+            collective_id=1, has_side_effects=True, vmem_limit_bytes=56 * 2**20
+        ),
+        name="experts",
+    )(info, normed, hidden1, gate, up, down, shared_gate, shared_up, shared_down)
 
 
 def body(
@@ -280,33 +510,13 @@
     running_count = jnp.dot(lower, one_hot, precision=lax.Precision.HIGHEST)
     slot_place = (jnp.sum(running_count * one_hot, axis=1) - 1.0).astype(jnp.int32)
     slot_index = flat_routes * capacity + slot_place
-    slot_total = expert_total * capacity
-    chosen = jnp.arange(slot_total, dtype=jnp.int32)[None, :, None] == slot_index.reshape(
-        rows_local, 1, top_count
-    )
-    placement = jnp.any(chosen, axis=2).astype(jnp.bfloat16)
-    weighted = jnp.sum(jnp.where(chosen, route_weight[:, None, :], 0.0), axis=2)
-    send_rows = lax.dot_general(
-        placement, normed, (((0,), (0,)), ((), ())), preferred_element_type=jnp.float32
-    ).astype(jnp.bfloat16)
-    send_rows = send_rows.reshape(expert_total, capacity, normed.shape[1])
-    shared_hidden = (
-        jax.nn.silu(jnp.dot(normed, shared_gate, preferred_element_type=jnp.float32))
-        * jnp.dot(normed, shared_up, preferred_element_type=jnp.float32)
-    ).astype(jnp.bfloat16)
-    shared_out = jnp.dot(shared_hidden, shared_down, preferred_element_type=jnp.float32)
-    processed = expert_apply(
-        lax.all_to_all(send_rows, ("sp", "tp"), split_axis=0, concat_axis=0, tiled=True),
-        expert_gate,
-        expert_up,
-        expert_down,
-    )
-    returned = lax.all_to_all(processed, ("sp", "tp"), split_axis=0, concat_axis=0, tiled=True)
-    returned = returned.reshape(slot_total, normed.shape[1])
-    mixed = shared_out + jnp.dot(
-        weighted.astype(jnp.bfloat16), returned, preferred_element_type=jnp.float32
-    )
-    return (hidden_f + mixed).astype(jnp.bfloat16)
+    slots = slot_index.reshape(rows_local, top_count).astype(jnp.float32)
+    info = jnp.concatenate([slots.T, route_weight.T], axis=0)
+    layer_out = routed_experts(
+        info, normed, hidden1, expert_gate, expert_up, expert_down,
+        shared_gate, shared_up, shared_down, capacity,
+    )
+    return layer_out.astype(jnp.bfloat16)
 
 
 def solution(mesh):

time: 269 us -> 197 us (0.73)
  Pallas kernels: 44.7 us -> 179 us
  blocking collectives: 97.2 us -> 0 us
  waiting for transfers between devices: 88.5 us -> 0 us
  matrix products: 26.6 us -> 5.13 us
  other arithmetic: 1.74 us -> 5.94 us
  starting transfers between devices: 3.79 us -> 0 us
    pallas_call x0 -> x1, Pallas kernels: none -> 135 us  [routed_experts(): pl.pallas_call(functools.partial(expert_kernel, n_sp, n_tp, planes, cap,...]
    all_to_all x1 -> x0, blocking collectives: 97.2 us -> none  [body(): lax.all_to_all(send_rows, ('sp', 'tp'), split_axis=0, concat_axis=0, tile...]
    all_to_all x1 -> x0, waiting for transfers between devices: 88.5 us -> none  [body(): lax.all_to_all(processed, ('sp', 'tp'), split_axis=0, concat_axis=0, tile...]
    dot_general x6 -> x0, matrix products: 21.6 us -> none  [the longest x1 9.06 us: expert_apply(): jnp.einsum('secf,efh->sech', hidden_e, expert_down, preferred_element_typ...]
    all_to_all x1 -> x0, starting transfers between devices: 3.79 us -> none  [body(): lax.all_to_all(processed, ('sp', 'tp'), split_axis=0, concat_axis=0, tile...]
  transfers between devices with their start and end apart: 1 -> 0, of which waited for: 1 -> 0; matrix products, arithmetic and copies ran while one was open for 2% -> 0% of each run, Pallas kernels for 0% -> 0%
where the time goes in v2:
time: 197 us; the launch traced here: 196 us
  Pallas kernels  179 us (91%)
  other arithmetic  5.94 us (3%)
  local copies, waits for them, and re-layouts  5.33 us (3%)
  matrix products  5.13 us (3%)
    pallas_call x1, Pallas kernels, routed_experts(): pl.pallas_call(functools.partial(expert_kernel, n_sp, n_tp, planes, cap,...  135 us
    pallas_call x1, Pallas kernels, attention(): pl.pallas_call(functools.partial(attention_kernel, mesh_sp, mesh_tp, plan...  44.7 us
    unnamed x15, local copies, waits for them, and re-layouts  4.95 us
    dot_general x1, matrix products, body(): projected = jnp.dot(all_heads, out_proj, preferred_element_type=jnp.float32)  4.85 us

profile of v2, /device:TPU:0, one launch (start us, length us, event | category | flops | bytes accessed | tf_op | source)
XLA Modules:
  0.0 196.0 jit_solution(3136591738333004805)
XLA Ops:
  0.0 0.1 multiply_sine_fusion.1
  0.1 0.2 multiply_sine_fusion
  0.4 0.8 copy.17
  1.2 0.1 eq.15
  1.3 0.3 fusion.1
  1.6 0.1 convert_element_type.44
  1.7 0.1 copy.18
  1.7 0.7 convert_bitcast_fusion
  2.4 1.3 pad_maximum_fusion.2.info_ref
  3.8 0.3 pad_maximum_fusion.1
  4.1 0.3 pad_maximum_fusion
  4.4 0.0 copy-start
  4.4 1.0 copy-done
  5.5 0.0 copy-start.1
  5.5 0.9 copy-done.1
  6.4 0.0 copy-start.2
  6.4 0.9 copy-done.2
  7.3 0.0 copy-start.3
  7.3 0.7 copy-done.3
  7.9 0.0 copy-start.4
  7.9 0.7 copy-done.4
  8.6 0.0 copy-start.6
  8.6 44.7 %attention.1 = bf16[128,2048]{1,0:T(8,128)(2,1)S(1)} custom-call(bf16[512,512]{1,0:T(8,128)(2,1)S(1)} %copy-done, bf16[512,128]{1,0:T(8,128)(2,1)S(1)} %copy-done.1, bf16[512,128]{1,0:T(8,128)(2,1)S(1)} %copy-done.2, f32[512,128]{1,0:T(8,128)S(1)} %bitcast.10, f32[512,128]{1,0:T(8,128)S(1)} %bitcast.9, f32[1,128]{1,0:T(1,128)S(1)} %bitcast.11, ...), custom_call_target="tpu_custom_call" | custom-call | tf_op jit(solution)/shard_map/attention/pallas_call | solution.py:203
  53.3 4.8 %fusion.2 = (f32[128]{0:T(128)S(1)}, bf16[128,2048]{1,0:T(8,128)(2,1)S(1)}) fusion(bf16[128,2048]{1,0:T(8,128)(2,1)S(1)} %attention.1, bf16[2048,2048]{1,0:T(8,128)(2,1)} %param.20, bf16[128,2048]{1,0:T(8,128)(2,1)} %param.19), kind=kOutput, calls=%fused_computation.6 | convolution fusion | flops 1075314560 | bytes 9961984 | tf_op jit(solution)/shard_map/dot_general | solution.py:492
  58.1 0.0 copy-start.5
  58.1 0.0 copy-done.6
  58.1 1.0 fusion.4.normed_ref
  59.1 0.0 copy-done.5
  59.1 134.8 %experts.1 = f32[128,2048]{1,0:T(8,128)} custom-call(f32[8,128]{1,0:T(8,128)} %pad_maximum_fusion.2.info_ref, bf16[128,2048]{1,0:T(8,128)(2,1)} %fusion.4.normed_ref, bf16[128,2048]{1,0:T(8,128)(2,1)} %copy-done.5, bf16[1,2048,256]{2,1,0:T(8,128)(2,1)} %gate_ref.1, bf16[1,2048,256]{2,1,0:T(8,128)(2,1)} %up_ref.1, bf16[1,256,2048]{2,1,0:T(8,128)(2,1)} %down_ref.1, ...), custom_call_target="tpu_custom_call" | custom-call | tf_op jit(solution)/shard_map/experts/pallas_call | solution.py:440
  193.9 2.1 %convert_element_type.52 = bf16[128,2048]{1,0:T(8,128)(2,1)} convert(f32[128,2048]{1,0:T(8,128)} %experts.1) | non-fusion elementwise | flops 262144 | bytes 1572864 | tf_op jit(solution)/shard_map/convert_element_type | solution.py:519
  (13 shorter events, 0.2 us)
Async XLA Ops:
  4.4 1.0 copy-start
  5.5 0.9 copy-start.1
  6.4 0.9 copy-start.2
  7.3 0.7 copy-start.3
  7.9 0.7 copy-start.4
  8.6 49.6 %copy-start.6 = (f32[2048]{0:T(1024)S(1)}, f32[2048]{0:T(1024)}, u32[]{:S(2)}) copy-start(f32[2048]{0:T(1024)} %param.23) | copy-start | bytes 24580
  58.1 1.0 copy-start.5

commit v3 on v2

--- a/solution.py
+++ b/solution.py
@@ -430,7 +430,7 @@
     rows, model = normed.shape
     planes = 4 if n_sp % 4 == 0 else 2
     team = n_sp // planes * n_tp
-    chunks = 4
+    chunks = 8
     wide = model // chunks
     slots = team * planes * cap
     inner = gate.shape[2]

time: 197 us -> 193 us (0.980)
  Pallas kernels: 179 us -> 176 us
    pallas_call x1, Pallas kernels: 135 us -> 131 us  [routed_experts(): pl.pallas_call(functools.partial(expert_kernel, n_sp, n_tp, planes, cap,...]
where the time goes in v3:
time: 193 us; the launch traced here: 192 us
  Pallas kernels  176 us (91%)
  other arithmetic  5.94 us (3%)
  local copies, waits for them, and re-layouts  5.33 us (3%)
  matrix products  5.13 us (3%)
    pallas_call x1, Pallas kernels, routed_experts(): pl.pallas_call(functools.partial(expert_kernel, n_sp, n_tp, planes, cap,...  131 us
    pallas_call x1, Pallas kernels, attention(): pl.pallas_call(functools.partial(attention_kernel, mesh_sp, mesh_tp, plan...  44.7 us
    unnamed x15, local copies, waits for them, and re-layouts  4.95 us
    dot_general x1, matrix products, body(): projected = jnp.dot(all_heads, out_proj, preferred_element_type=jnp.float32)  4.85 us

profile of v3, /device:TPU:0, one launch (start us, length us, event | category | flops | bytes accessed | tf_op | source)
XLA Modules:
  0.0 192.5 jit_solution(4489501114574195487)
XLA Ops:
  0.0 0.1 multiply_sine_fusion.1
  0.1 0.2 multiply_sine_fusion
  0.4 0.8 copy.17
  1.2 0.1 eq.15
  1.3 0.3 fusion.1
  1.6 0.1 convert_element_type.44
  1.7 0.1 copy.18
  1.7 0.7 convert_bitcast_fusion
  2.4 1.3 pad_maximum_fusion.2.info_ref
  3.8 0.3 pad_maximum_fusion.1
  4.1 0.3 pad_maximum_fusion
  4.4 0.0 copy-start
  4.4 1.0 copy-done
  5.5 0.0 copy-start.1
  5.5 0.9 copy-done.1
  6.4 0.0 copy-start.2
  6.4 0.9 copy-done.2
  7.3 0.0 copy-start.3
  7.3 0.7 copy-done.3
  7.9 0.0 copy-start.4
  7.9 0.7 copy-done.4
  8.6 0.0 copy-start.6
  8.6 44.7 %attention.1 = bf16[128,2048]{1,0:T(8,128)(2,1)S(1)} custom-call(bf16[512,512]{1,0:T(8,128)(2,1)S(1)} %copy-done, bf16[512,128]{1,0:T(8,128)(2,1)S(1)} %copy-done.1, bf16[512,128]{1,0:T(8,128)(2,1)S(1)} %copy-done.2, f32[512,128]{1,0:T(8,128)S(1)} %bitcast.10, f32[512,128]{1,0:T(8,128)S(1)} %bitcast.9, f32[1,128]{1,0:T(1,128)S(1)} %bitcast.11, ...), custom_call_target="tpu_custom_call" | custom-call | tf_op jit(solution)/shard_map/attention/pallas_call | solution.py:203
  53.3 4.8 %fusion.2 = (f32[128]{0:T(128)S(1)}, bf16[128,2048]{1,0:T(8,128)(2,1)S(1)}) fusion(bf16[128,2048]{1,0:T(8,128)(2,1)S(1)} %attention.1, bf16[2048,2048]{1,0:T(8,128)(2,1)} %param.20, bf16[128,2048]{1,0:T(8,128)(2,1)} %param.19), kind=kOutput, calls=%fused_computation.6 | convolution fusion | flops 1075314560 | bytes 9961984 | tf_op jit(solution)/shard_map/dot_general | solution.py:492
  58.1 0.0 copy-start.5
  58.1 0.0 copy-done.6
  58.1 1.0 fusion.4.normed_ref
  59.1 0.0 copy-done.5
  59.1 131.2 %experts.1 = f32[128,2048]{1,0:T(8,128)} custom-call(f32[8,128]{1,0:T(8,128)} %pad_maximum_fusion.2.info_ref, bf16[128,2048]{1,0:T(8,128)(2,1)} %fusion.4.normed_ref, bf16[128,2048]{1,0:T(8,128)(2,1)} %copy-done.5, bf16[1,2048,256]{2,1,0:T(8,128)(2,1)} %gate_ref.1, bf16[1,2048,256]{2,1,0:T(8,128)(2,1)} %up_ref.1, bf16[1,256,2048]{2,1,0:T(8,128)(2,1)} %down_ref.1, ...), custom_call_target="tpu_custom_call" | custom-call | tf_op jit(solution)/shard_map/experts/pallas_call | solution.py:440
  190.4 2.1 %convert_element_type.52 = bf16[128,2048]{1,0:T(8,128)(2,1)} convert(f32[128,2048]{1,0:T(8,128)} %experts.1) | non-fusion elementwise | flops 262144 | bytes 1572864 | tf_op jit(solution)/shard_map/convert_element_type | solution.py:519
  (13 shorter events, 0.2 us)
Async XLA Ops:
  4.4 1.0 copy-start
  5.5 0.9 copy-start.1
  6.4 0.9 copy-start.2
  7.3 0.7 copy-start.3
  7.9 0.7 copy-start.4
  8.6 49.6 %copy-start.6 = (f32[2048]{0:T(1024)S(1)}, f32[2048]{0:T(1024)}, u32[]{:S(2)}) copy-start(f32[2048]{0:T(1024)} %param.23) | copy-start | bytes 24580
  58.1 1.0 copy-start.5
